TPU v7x, 32 devices: a whole 2x2x4 slice. The times are simulated.
32 devices in a mesh: row: 4 (over y, x), col: 8 (over z, core).
Axes of the slice: x: 2, y: 2, z: 4, core: 2. Of those that a mesh axis runs over, the one named last changes fastest.
Arguments:
- tokens: bfloat16 [2, 2048, 1024], P(None, ('row', 'col')), may hold values from -6 to 6
- proj_weight: bfloat16 [1024, 256], replicated, may hold values from -0.1875 to 0.1875
- gate_weight: bfloat16 [1024, 256], replicated, may hold values from -0.1875 to 0.1875
- out_weight: bfloat16 [256, 1024], replicated, may hold values from -0.375 to 0.375
Outputs:
- mixed_out: bfloat16 [2, 2048, 1024], P(None, ('col', 'row'))
All inputs are finite; a program needn't handle non-finite values.
Results may differ from a plain program's by a relative error of at most 0.02.
Values may be sent and summed in bfloat16 or wider, within the bound.
A program may use at most 64 MiB of HBM per device.

v0:
```python
import math
import jax
import jax.numpy as jnp
from jax import lax
from jax.sharding import PartitionSpec as P

GROUPS = 4
GROUP_DIM = 64


def as_sent(x):
    return jax.tree.map(lambda a: a.astype(jnp.bfloat16) if a.dtype == jnp.float32 else a, x)


def channel_tables(table_size):
    index_vec = jnp.arange(table_size, dtype=jnp.int32)
    turns_mod = index_vec[:, None] * index_vec[None, :] % table_size
    angles = 2.0 * math.pi / table_size * turns_mod.astype(jnp.float32)
    norm_scale = 1.0 / math.sqrt(table_size)
    return (jnp.cos(angles) * norm_scale, jnp.sin(angles) * norm_scale)


def channel_section(mix_input):
    seq_count, tok_rows = (mix_input.shape[0], mix_input.shape[1])
    grouped = mix_input.astype(jnp.float32).reshape(seq_count, tok_rows, GROUPS, GROUP_DIM)
    cos_table, sin_table = channel_tables(GROUP_DIM)
    real_part = jnp.einsum("stgn,nk->tsgk", grouped, cos_table, precision=lax.Precision.HIGHEST)
    imag_part = -jnp.einsum("stgn,nk->tsgk", grouped, sin_table, precision=lax.Precision.HIGHEST)
    return (real_part.reshape(tok_rows, -1), imag_part.reshape(tok_rows, -1))


def row_factor(real_part, imag_part, col_start, length_all):
    row_count, tok_rows, col_width = real_part.shape
    cos_table, sin_table = channel_tables(row_count)
    cos_table = cos_table * math.sqrt(row_count)
    sin_table = sin_table * math.sqrt(row_count)
    high = lax.Precision.HIGHEST
    first_real = jnp.einsum("ka,atm->ktm", cos_table, real_part, precision=high) + jnp.einsum(
        "ka,atm->ktm", sin_table, imag_part, precision=high
    )
    first_imag = jnp.einsum("ka,atm->ktm", cos_table, imag_part, precision=high) - jnp.einsum(
        "ka,atm->ktm", sin_table, real_part, precision=high
    )
    index_vec = jnp.arange(row_count, dtype=jnp.int32)
    position = col_start + jnp.arange(tok_rows, dtype=jnp.int32)
    turns_mod = index_vec[:, None] * position[None, :] % length_all
    angles = 2.0 * math.pi / length_all * turns_mod.astype(jnp.float32)
    twiddle_cos = jnp.cos(angles)[:, :, None]
    twiddle_sin = jnp.sin(angles)[:, :, None]
    turned_real = twiddle_cos * first_real + twiddle_sin * first_imag
    turned_imag = twiddle_cos * first_imag - twiddle_sin * first_real
    merged_real = jnp.transpose(turned_real, (1, 0, 2)).reshape(tok_rows, row_count * col_width)
    merged_imag = jnp.transpose(turned_imag, (1, 0, 2)).reshape(tok_rows, row_count * col_width)
    return (merged_real, merged_imag)


def dense_section(real_part, imag_part, length_all):
    length = real_part.shape[0]
    block_rows = min(512, length)
    block_count = length // block_rows
    points = jnp.arange(length, dtype=jnp.int32)

    def one_block(block_start):
        freq_index = block_start + jnp.arange(block_rows, dtype=jnp.int32)
        turns_mod = freq_index[:, None] * points[None, :] % length
        angles = 2.0 * math.pi / length * turns_mod.astype(jnp.float32)
        first = jnp.dot(
            jnp.cos(angles),
            real_part,
            precision=lax.Precision.HIGHEST,
            preferred_element_type=jnp.float32,
        )
        second = jnp.dot(
            jnp.sin(angles),
            imag_part,
            precision=lax.Precision.HIGHEST,
            preferred_element_type=jnp.float32,
        )
        return first + second

    starts = jnp.arange(block_count, dtype=jnp.int32) * block_rows
    spectrum = lax.map(one_block, starts).reshape(length, real_part.shape[1])
    return (spectrum * (1.0 / math.sqrt(length_all))).astype(jnp.bfloat16)


def local_order(returned, row_count):
    tok_rows = returned.shape[0]
    return returned.reshape(tok_rows, row_count, -1).reshape(tok_rows * row_count, -1)


def body(tokens, proj_weight, gate_weight, out_weight):
    seq_count, tok_rows, model_width = tokens.shape
    flattened = tokens.reshape(seq_count * tok_rows, model_width)
    hidden = jnp.dot(flattened, proj_weight, preferred_element_type=jnp.float32).astype(
        jnp.bfloat16
    )
    gate_pre = jnp.dot(flattened, gate_weight, preferred_element_type=jnp.float32)
    mix_input = (hidden.astype(jnp.float32) * jax.nn.silu(gate_pre)).astype(jnp.bfloat16)
    real_part, imag_part = channel_section(mix_input.reshape(seq_count, tok_rows, -1))
    row_count = lax.axis_size("row")
    length_all = row_count * lax.axis_size("col") * tok_rows
    col_start = lax.axis_index("col") * tok_rows
    received = (
        lax.all_to_all(as_sent(real_part[None]), "row", split_axis=2, concat_axis=0, tiled=True),
        lax.all_to_all(as_sent(imag_part[None]), "row", split_axis=2, concat_axis=0, tiled=True),
    )
    merged_real, merged_imag = row_factor(received[0], received[1], col_start, length_all)
    moved_pair = (
        lax.all_to_all(as_sent(merged_real), "col", split_axis=1, concat_axis=0, tiled=True).astype(
            merged_real.dtype
        ),
        lax.all_to_all(as_sent(merged_imag), "col", split_axis=1, concat_axis=0, tiled=True).astype(
            merged_imag.dtype
        ),
    )
    spectrum = dense_section(moved_pair[0], moved_pair[1], length_all)
    returned = lax.all_to_all(spectrum, "col", split_axis=0, concat_axis=1, tiled=True)
    mixed_cols = lax.all_to_all(
        local_order(returned, row_count), "row", split_axis=0, concat_axis=1, tiled=True
    )
    mixed = mixed_cols.reshape(tok_rows, seq_count, -1)
    result_out = jnp.einsum("tsc,cd->std", mixed, out_weight, preferred_element_type=jnp.float32)
    return result_out.astype(jnp.bfloat16)


def solution(mesh):
    in_specs = (P(None, ("row", "col"), None), P(), P(), P())
    out_specs = P(None, ("col", "row"), None)
    return jax.shard_map(body, mesh=mesh, in_specs=in_specs, out_specs=out_specs, check_vma=False)
```

profile of v0, /device:TPU:0, one launch (start us, length us, event | category | flops | bytes accessed | tf_op | source)
XLA Modules:
  0.0 73.2 jit_solution(7594770349935760409)
XLA Ops:
  0.0 0.0 copy-start
  0.0 0.0 copy-start.2
  0.0 0.0 copy-start.1
  0.0 1.5 %fusion.98 = f32[128,256]{1,0:T(8,128)S(1)} fusion(bf16[128,1024]{1,0:T(8,128)(2,1)} %bitcast.95, bf16[1024,256]{1,0:T(8,128)(2,1)} %param.6), kind=kOutput, calls=%fused_computation.116 | convolution fusion | flops 67108864 | bytes 917504 | tf_op jit(solution)/shard_map/dot_general | solution.py:97
  1.5 0.0 copy-done.2
  1.5 0.0 copy-done.1
  1.5 0.2 fusion.8
  1.7 0.1 reshape.121
  1.9 0.6 convolution_convert_fusion.1
  2.4 0.2 copy.62
  2.6 0.5 broadcast.201
  3.1 1.4 %reduce.1 = bf16[512,64]{1,0:T(8,128)(2,1)S(1)} reduce(bf16[512,1,64]{2,1,0:T(2,128)(2,1)S(1)} %bitcast.89, bf16[]{:T(256)} %broadcast.201), dimensions={1}, to_apply=%bitcast.86.reduce_sub_computation | reduce | bytes 131074
  4.6 0.8 %reshape.130 = bf16[4,2,4096]{2,1,0:T(2,128)(2,1)} reshape(bf16[512,64]{1,0:T(8,128)(2,1)S(1)} %reduce.1) | data formatting | bytes 131072
  5.4 5.2 %all-to-all-start = ((bf16[4,2,4096]{2,1,0:T(2,128)(2,1)}), bf16[4,2,4096]{2,1,0:T(2,128)(2,1)S(1)}, u32[]{:S(2)}, u32[]{:S(2)}) async-start(bf16[4,2,4096]{2,1,0:T(2,128)(2,1)} %reshape.130), calls=%async_computation | async-start | bytes 131072 | tf_op jit(solution)/shard_map/all_to_all | solution.py:104
  10.6 0.6 fusion.1
  11.1 0.1 fusion.63
  11.2 0.1 copy.32
  11.3 0.1 copy.39
  11.4 0.2 copy.61
  11.6 1.4 %reduce = bf16[512,64]{1,0:T(8,128)(2,1)S(1)} reduce(bf16[512,1,64]{2,1,0:T(2,128)(2,1)S(1)} %bitcast.90, bf16[]{:T(256)} %broadcast.201), dimensions={1}, to_apply=%bitcast.85.reduce_sub_computation | reduce | bytes 131074
  13.1 0.8 %reshape.128 = bf16[4,2,4096]{2,1,0:T(2,128)(2,1)} reshape(bf16[512,64]{1,0:T(8,128)(2,1)S(1)} %reduce) | data formatting | bytes 131072
  13.9 1.6 %all-to-all-done = bf16[4,2,4096]{2,1,0:T(2,128)(2,1)S(1)} async-done(((bf16[4,2,4096]{2,1,0:T(2,128)(2,1)}), bf16[4,2,4096]{2,1,0:T(2,128)(2,1)S(1)}, u32[]{:S(2)}, u32[]{:S(2)}) %all-to-all-start) | async-done | bytes 65568 | tf_op jit(solution)/shard_map/all_to_all | solution.py:104
  15.4 3.3 %all-to-all-start.1 = ((bf16[4,2,4096]{2,1,0:T(2,128)(2,1)}), bf16[4,2,4096]{2,1,0:T(2,128)(2,1)S(1)}, u32[]{:S(2)}, u32[]{:S(2)}) async-start(bf16[4,2,4096]{2,1,0:T(2,128)(2,1)} %reshape.128), calls=%async_computation.1 | async-start | bytes 131072 | tf_op jit(solution)/shard_map/all_to_all | solution.py:105
  18.7 0.1 reshape.131
  18.9 0.1 copy.35
  19.0 0.3 fusion.24
  19.3 4.2 %all-to-all-done.1 = bf16[4,2,4096]{2,1,0:T(2,128)(2,1)S(1)} async-done(((bf16[4,2,4096]{2,1,0:T(2,128)(2,1)}), bf16[4,2,4096]{2,1,0:T(2,128)(2,1)S(1)}, u32[]{:S(2)}, u32[]{:S(2)}) %all-to-all-start.1) | async-done | bytes 65568 | tf_op jit(solution)/shard_map/all_to_all | solution.py:105
  23.5 0.1 reshape.129
  23.7 0.1 copy.38
  23.8 0.3 fusion.26
  24.1 0.3 fusion.2
  24.5 0.4 subtract_convert_fusion
  24.8 0.1 copy.51
  25.0 0.8 %reshape.134 = bf16[8,2,2048]{2,1,0:T(2,128)(2,1)} reshape(bf16[8,64,64]{2,1,0:T(8,128)(2,1)S(1)} %bitcast.91) | data formatting | bytes 131072
  25.8 4.9 %all-to-all-start.3 = ((bf16[8,2,2048]{2,1,0:T(2,128)(2,1)}), bf16[8,2,2048]{2,1,0:T(2,128)(2,1)S(1)}, u32[]{:S(2)}, u32[]{:S(2)}) async-start(bf16[8,2,2048]{2,1,0:T(2,128)(2,1)} %reshape.134), calls=%async_computation.3 | async-start | bytes 131072 | tf_op jit(solution)/shard_map/all_to_all | solution.py:112
  30.6 0.1 copy.50
  30.8 0.8 %reshape.132 = bf16[8,2,2048]{2,1,0:T(2,128)(2,1)} reshape(bf16[8,64,64]{2,1,0:T(8,128)(2,1)S(1)} %bitcast.92) | data formatting | bytes 131072
  31.6 5.0 %all-to-all-done.3 = bf16[8,2,2048]{2,1,0:T(2,128)(2,1)S(1)} async-done(((bf16[8,2,2048]{2,1,0:T(2,128)(2,1)}), bf16[8,2,2048]{2,1,0:T(2,128)(2,1)S(1)}, u32[]{:S(2)}, u32[]{:S(2)}) %all-to-all-start.3) | async-done | bytes 65568 | tf_op jit(solution)/shard_map/all_to_all | solution.py:112
  36.6 3.4 %all-to-all-start.2 = ((bf16[8,2,2048]{2,1,0:T(2,128)(2,1)}), bf16[8,2,2048]{2,1,0:T(2,128)(2,1)S(1)}, u32[]{:S(2)}, u32[]{:S(2)}) async-start(bf16[8,2,2048]{2,1,0:T(2,128)(2,1)} %reshape.132), calls=%async_computation.2 | async-start | bytes 131072 | tf_op jit(solution)/shard_map/all_to_all | solution.py:109
  39.9 0.1 reshape.135
  40.1 0.1 copy.43
  40.2 0.1 all_to_all.85
  40.3 5.4 %all-to-all-done.2 = bf16[8,2,2048]{2,1,0:T(2,128)(2,1)S(1)} async-done(((bf16[8,2,2048]{2,1,0:T(2,128)(2,1)}), bf16[8,2,2048]{2,1,0:T(2,128)(2,1)S(1)}, u32[]{:S(2)}, u32[]{:S(2)}) %all-to-all-start.2) | async-done | bytes 65568 | tf_op jit(solution)/shard_map/all_to_all | solution.py:109
  45.8 0.1 reshape.133
  45.9 0.1 copy.41
  46.0 0.1 all_to_all.82
  46.2 4.7 %fusion.13 = f32[512,64]{0,1:T(8,128)S(1)} fusion(bf16[512,64]{0,1:T(8,128)(2,1)S(1)} %all_to_all.82), kind=kOutput, calls=%fused_computation.23 | convolution fusion | flops 204996608 | bytes 196608 | tf_op jit(solution)/shard_map/while/body/eval_jaxpr/dot_general | solution.py:67
  50.9 5.1 %fusion.5 = bf16[512,64]{0,1:T(8,128)(2,1)S(1)} fusion(f32[512,64]{0,1:T(8,128)S(1)} %fusion.13, bf16[512,64]{0,1:T(8,128)(2,1)S(1)} %all_to_all.85), kind=kOutput, calls=%fused_computation.14 | convolution fusion | flops 205094912 | bytes 262144 | tf_op jit(solution)/shard_map/while/body/eval_jaxpr/dot_general | solution.py:73
  56.0 0.1 copy.52
  56.1 0.2 reshape.136
  56.3 8.3 %all_to_all.97 = bf16[8,2,2048]{2,1,0:T(2,128)(2,1)S(1)} all-to-all(bf16[8,2,2048]{2,1,0:T(2,128)(2,1)S(1)} %reshape.136), channel_id=1, replica_groups=mesh['row'=4,'col'=8] {'col'}, dimensions={0} | all-to-all | bytes 131072 | tf_op jit(solution)/shard_map/all_to_all | solution.py:117
  64.6 0.1 reshape.137
  64.8 0.1 copy.45
  64.8 0.1 all_to_all.88
  65.0 7.2 %all_to_all.98 = bf16[4,64,128]{2,1,0:T(8,128)(2,1)S(1)} all-to-all(bf16[4,64,128]{2,1,0:T(8,128)(2,1)S(1)} %all_to_all.88), channel_id=1, replica_groups=mesh['row'=4,'col'=8] {'row'}, dimensions={0} | all-to-all | bytes 131072 | tf_op jit(solution)/shard_map/all_to_all | solution.py:118
  72.2 0.1 copy.46
  72.3 0.0 copy-done
  72.3 0.9 %fusion = bf16[2,64,1024]{2,1,0:T(8,128)(2,1)} fusion(bf16[256,1024]{1,0:T(8,128)(2,1)S(1)} %copy-done, bf16[64,2,256]{2,1,0:T(2,128)(2,1)S(1)} %reshape.122), kind=kOutput, calls=%fused_computation.4 | convolution fusion | flops 67239936 | bytes 851968 | tf_op jit(solution)/shard_map/tsc,cd->std/dot_general | solution.py:122
  (6 shorter events, 0.1 us)
Async XLA Ops:
  0.0 72.3 %copy-start = (bf16[256,1024]{1,0:T(8,128)(2,1)S(1)}, bf16[256,1024]{1,0:T(8,128)(2,1)}, u32[]{:S(2)}) copy-start(bf16[256,1024]{1,0:T(8,128)(2,1)} %param.7) | copy-start | bytes 1572868
  0.0 1.5 %copy-start.2 = (bf16[1024,256]{1,0:T(8,128)(2,1)S(1)}, bf16[1024,256]{1,0:T(8,128)(2,1)}, u32[]{:S(2)}) copy-start(bf16[1024,256]{1,0:T(8,128)(2,1)} %param.5) | copy-start | bytes 1572868
  0.0 1.5 %copy-start.1 = (bf16[2,64,1024]{2,1,0:T(8,128)(2,1)S(1)}, bf16[2,64,1024]{2,1,0:T(8,128)(2,1)}, u32[]{:S(2)}) copy-start(bf16[2,64,1024]{2,1,0:T(8,128)(2,1)} %param.4) | copy-start | bytes 786436
  5.4 10.0 %all-to-all-start = ((bf16[4,2,4096]{2,1,0:T(2,128)(2,1)}), bf16[4,2,4096]{2,1,0:T(2,128)(2,1)S(1)}, u32[]{:S(2)}, u32[]{:S(2)}) async-start(bf16[4,2,4096]{2,1,0:T(2,128)(2,1)} %reshape.130), calls=%async_computation | async-start | bytes 131072 | tf_op jit(solution)/shard_map/all_to_all | solution.py:104
  15.4 8.1 %all-to-all-start.1 = ((bf16[4,2,4096]{2,1,0:T(2,128)(2,1)}), bf16[4,2,4096]{2,1,0:T(2,128)(2,1)S(1)}, u32[]{:S(2)}, u32[]{:S(2)}) async-start(bf16[4,2,4096]{2,1,0:T(2,128)(2,1)} %reshape.128), calls=%async_computation.1 | async-start | bytes 131072 | tf_op jit(solution)/shard_map/all_to_all | solution.py:105
  25.8 10.8 %all-to-all-start.3 = ((bf16[8,2,2048]{2,1,0:T(2,128)(2,1)}), bf16[8,2,2048]{2,1,0:T(2,128)(2,1)S(1)}, u32[]{:S(2)}, u32[]{:S(2)}) async-start(bf16[8,2,2048]{2,1,0:T(2,128)(2,1)} %reshape.134), calls=%async_computation.3 | async-start | bytes 131072 | tf_op jit(solution)/shard_map/all_to_all | solution.py:112
  36.6 9.2 %all-to-all-start.2 = ((bf16[8,2,2048]{2,1,0:T(2,128)(2,1)}), bf16[8,2,2048]{2,1,0:T(2,128)(2,1)S(1)}, u32[]{:S(2)}, u32[]{:S(2)}) async-start(bf16[8,2,2048]{2,1,0:T(2,128)(2,1)} %reshape.132), calls=%async_computation.2 | async-start | bytes 131072 | tf_op jit(solution)/shard_map/all_to_all | solution.py:109
where the time goes:
time: 73.9 us; the launch traced here: 73.2 us
  starting transfers between devices  16.7 us (23%)
  waiting for transfers between devices  16.2 us (22%)
  blocking collectives  15.5 us (21%)
  matrix products  14.9 us (20%)
  local copies, waits for them, and re-layouts  6.73 us (9%)
  other arithmetic  2.94 us (4%)
    all_to_all x1, blocking collectives, body(): lax.all_to_all(spectrum, 'col', split_axis=0, concat_axis=1, tiled=True)  8.3 us
    all_to_all x1, blocking collectives, body(): lax.all_to_all(local_order(returned, row_count), 'row', split_axis=0, con...  7.21 us
    all_to_all x1, waiting for transfers between devices, body(): lax.all_to_all(as_sent(merged_real), 'col', split_axis=1, concat_axis=0,...  5.44 us
    all_to_all x1, starting transfers between devices, body(): lax.all_to_all(as_sent(real_part[None]), 'row', split_axis=2, concat_axis...  5.2 us
    dot_general x1, matrix products, one_block(): jnp.dot(jnp.sin(angles), imag_part, precision=lax.Precision.HIGHEST, pref...  5.11 us
    all_to_all x1, waiting for transfers between devices, body(): lax.all_to_all(as_sent(merged_imag), 'col', split_axis=1, concat_axis=0,...  4.98 us
    all_to_all x1, starting transfers between devices, body(): lax.all_to_all(as_sent(merged_imag), 'col', split_axis=1, concat_axis=0,...  4.88 us
    dot_general x1, matrix products, one_block(): jnp.dot(jnp.cos(angles), real_part, precision=lax.Precision.HIGHEST, pref...  4.73 us
  transfers between devices with their start and end apart: 4, of which 4 were waited for; matrix products, arithmetic and copies ran while one was open for 7% of the time, Pallas kernels for 0%

commit v1 on v0

--- a/solution.py
+++ b/solution.py
@@ -6,6 +6,13 @@
 
 GROUPS = 4
 GROUP_DIM = 64
+
+
+def stacked_exchange(value, axis, split, join):
+    size = lax.axis_size(axis)
+    blocks = jnp.stack(jnp.split(value, size, axis=split), axis=0)
+    blocks = lax.all_to_all(blocks, axis, split_axis=0, concat_axis=0)
+    return jnp.concatenate(blocks, axis=join)
 
 
 def as_sent(x):
@@ -109,9 +116,7 @@
         lax.all_to_all(as_sent(merged_real), "col", split_axis=1, concat_axis=0, tiled=True).astype(
             merged_real.dtype
         ),
-        lax.all_to_all(as_sent(merged_imag), "col", split_axis=1, concat_axis=0, tiled=True).astype(
-            merged_imag.dtype
-        ),
+        stacked_exchange(as_sent(merged_imag), "col", 1, 0).astype(merged_imag.dtype),
     )
     spectrum = dense_section(moved_pair[0], moved_pair[1], length_all)
     returned = lax.all_to_all(spectrum, "col", split_axis=0, concat_axis=1, tiled=True)

time: 73.9 us -> 70.6 us (0.955)
  waiting for transfers between devices: 16.2 us -> 11.5 us
  blocking collectives: 15.5 us -> 17.3 us
    all_to_all x1, waiting for transfers between devices: 4.98 us -> 0.71 us  [stacked_exchange(): blocks = lax.all_to_all(blocks, axis, split_axis=0, concat_axis=0)]
    all_to_all x1, blocking collectives: 8.3 us -> 10 us  [body(): lax.all_to_all(spectrum, 'col', split_axis=0, concat_axis=1, tiled=True)]
    all_to_all x1, starting transfers between devices: 4.88 us -> 3.35 us  [stacked_exchange(): blocks = lax.all_to_all(blocks, axis, split_axis=0, concat_axis=0)]
    all_to_all x1, starting transfers between devices: 3.35 us -> 4.88 us  [body(): lax.all_to_all(as_sent(merged_real), 'col', split_axis=1, concat_axis=0,...]
    unnamed x17 -> x25, local copies, waits for them, and re-layouts: 4.56 us -> 4.86 us
  transfers between devices with their start and end apart: 4 -> 4, of which waited for: 4 -> 4; matrix products, arithmetic and copies ran while one was open for 7% -> 14% of each run, Pallas kernels for 0% -> 0%
where the time goes in v1:
time: 70.6 us; the launch traced here: 70 us
  blocking collectives  17.3 us (25%)
  starting transfers between devices  16.7 us (24%)
  matrix products  14.5 us (21%)
  waiting for transfers between devices  11.5 us (16%)
  local copies, waits for them, and re-layouts  6.73 us (10%)
  other arithmetic  2.94 us (4%)
    all_to_all x1, blocking collectives, body(): lax.all_to_all(spectrum, 'col', split_axis=0, concat_axis=1, tiled=True)  10 us
    all_to_all x1, blocking collectives, body(): lax.all_to_all(local_order(returned, row_count), 'row', split_axis=0, con...  7.21 us
    all_to_all x1, starting transfers between devices, body(): lax.all_to_all(as_sent(real_part[None]), 'row', split_axis=2, concat_axis...  5.2 us
    all_to_all x1, waiting for transfers between devices, body(): lax.all_to_all(as_sent(merged_real), 'col', split_axis=1, concat_axis=0,...  5.05 us
    all_to_all x1, starting transfers between devices, body(): lax.all_to_all(as_sent(merged_real), 'col', split_axis=1, concat_axis=0,...  4.88 us
    unnamed x25, local copies, waits for them, and re-layouts  4.86 us
    dot_general x1, matrix products, one_block(): jnp.dot(jnp.cos(angles), real_part, precision=lax.Precision.HIGHEST, pref...  4.73 us
    dot_general x1, matrix products, one_block(): jnp.dot(jnp.sin(angles), imag_part, precision=lax.Precision.HIGHEST, pref...  4.72 us
  transfers between devices with their start and end apart: 4, of which 4 were waited for; matrix products, arithmetic and copies ran while one was open for 14% of the time, Pallas kernels for 0%

profile of v1, /device:TPU:0, one launch (start us, length us, event | category | flops | bytes accessed | tf_op | source)
XLA Modules:
  0.0 70.0 jit_solution(6068337550654276730)
XLA Ops:
  0.0 0.0 copy-start
  0.0 0.0 copy-start.2
  0.0 0.0 copy-start.1
  0.0 1.5 %fusion.98 = f32[128,256]{1,0:T(8,128)S(1)} fusion(bf16[128,1024]{1,0:T(8,128)(2,1)} %bitcast.131, bf16[1024,256]{1,0:T(8,128)(2,1)} %param.6), kind=kOutput, calls=%fused_computation.132 | convolution fusion | flops 67108864 | bytes 917504 | tf_op jit(solution)/shard_map/dot_general | solution.py:104
  1.5 0.0 copy-done.2
  1.5 0.0 copy-done.1
  1.5 0.2 fusion.8
  1.7 0.1 reshape.120
  1.9 0.6 convolution_convert_fusion.1
  2.4 0.2 copy.59
  2.6 0.5 broadcast.201
  3.1 1.4 %reduce.1 = bf16[512,64]{1,0:T(8,128)(2,1)S(1)} reduce(bf16[512,1,64]{2,1,0:T(2,128)(2,1)S(1)} %bitcast.118, bf16[]{:T(256)} %broadcast.201), dimensions={1}, to_apply=%bitcast.115.reduce_sub_computation | reduce | bytes 131074
  4.6 0.8 %reshape.130 = bf16[4,2,4096]{2,1,0:T(2,128)(2,1)} reshape(bf16[512,64]{1,0:T(8,128)(2,1)S(1)} %reduce.1) | data formatting | bytes 131072
  5.4 5.2 %all-to-all-start = ((bf16[4,2,4096]{2,1,0:T(2,128)(2,1)}), bf16[4,2,4096]{2,1,0:T(2,128)(2,1)S(1)}, u32[]{:S(2)}, u32[]{:S(2)}) async-start(bf16[4,2,4096]{2,1,0:T(2,128)(2,1)} %reshape.130), calls=%async_computation | async-start | bytes 131072 | tf_op jit(solution)/shard_map/all_to_all | solution.py:111
  10.6 0.6 fusion.1
  11.1 0.1 fusion.63
  11.2 0.1 copy.29
  11.3 0.1 copy.36
  11.4 0.2 copy.58
  11.6 1.4 %reduce = bf16[512,64]{1,0:T(8,128)(2,1)S(1)} reduce(bf16[512,1,64]{2,1,0:T(2,128)(2,1)S(1)} %bitcast.119, bf16[]{:T(256)} %broadcast.201), dimensions={1}, to_apply=%bitcast.114.reduce_sub_computation | reduce | bytes 131074
  13.1 0.8 %reshape.128 = bf16[4,2,4096]{2,1,0:T(2,128)(2,1)} reshape(bf16[512,64]{1,0:T(8,128)(2,1)S(1)} %reduce) | data formatting | bytes 131072
  13.9 1.6 %all-to-all-done = bf16[4,2,4096]{2,1,0:T(2,128)(2,1)S(1)} async-done(((bf16[4,2,4096]{2,1,0:T(2,128)(2,1)}), bf16[4,2,4096]{2,1,0:T(2,128)(2,1)S(1)}, u32[]{:S(2)}, u32[]{:S(2)}) %all-to-all-start) | async-done | bytes 65568 | tf_op jit(solution)/shard_map/all_to_all | solution.py:111
  15.4 3.3 %all-to-all-start.1 = ((bf16[4,2,4096]{2,1,0:T(2,128)(2,1)}), bf16[4,2,4096]{2,1,0:T(2,128)(2,1)S(1)}, u32[]{:S(2)}, u32[]{:S(2)}) async-start(bf16[4,2,4096]{2,1,0:T(2,128)(2,1)} %reshape.128), calls=%async_computation.1 | async-start | bytes 131072 | tf_op jit(solution)/shard_map/all_to_all | solution.py:112
  18.7 0.1 reshape.131
  18.9 0.1 copy.32
  19.0 0.3 fusion.24
  19.3 4.2 %all-to-all-done.1 = bf16[4,2,4096]{2,1,0:T(2,128)(2,1)S(1)} async-done(((bf16[4,2,4096]{2,1,0:T(2,128)(2,1)}), bf16[4,2,4096]{2,1,0:T(2,128)(2,1)S(1)}, u32[]{:S(2)}, u32[]{:S(2)}) %all-to-all-start.1) | async-done | bytes 65568 | tf_op jit(solution)/shard_map/all_to_all | solution.py:112
  23.5 0.1 reshape.129
  23.7 0.1 copy.35
  23.8 0.3 fusion.26
  24.1 0.3 fusion.2
  24.5 0.4 subtract_convert_fusion
  24.9 0.1 constant_dynamic-update-slice_fusion.6
  25.0 0.1 constant_dynamic-update-slice_fusion.4
  25.1 0.1 constant_dynamic-update-slice_fusion.2
  25.2 0.1 copy.45
  25.3 0.8 %reshape.132 = bf16[8,2,2048]{2,1,0:T(2,128)(2,1)} reshape(bf16[8,64,64]{2,1,0:T(8,128)(2,1)S(1)} %bitcast.128) | data formatting | bytes 131072
  26.1 4.9 %all-to-all-start.2 = ((bf16[8,2,2048]{2,1,0:T(2,128)(2,1)}), bf16[8,2,2048]{2,1,0:T(2,128)(2,1)S(1)}, u32[]{:S(2)}, u32[]{:S(2)}) async-start(bf16[8,2,2048]{2,1,0:T(2,128)(2,1)} %reshape.132), calls=%async_computation.2 | async-start | bytes 131072 | tf_op jit(solution)/shard_map/all_to_all | solution.py:116
  31.0 0.1 constant_dynamic-update-slice_fusion
  31.1 0.8 %reshape.134 = bf16[8,2,2048]{2,1,0:T(2,128)(2,1)} reshape(bf16[8,64,64]{2,1,0:T(8,128)(2,1)S(1)} %constant_dynamic-update-slice_fusion) | data formatting | bytes 131072
  31.8 5.1 %all-to-all-done.2 = bf16[8,2,2048]{2,1,0:T(2,128)(2,1)S(1)} async-done(((bf16[8,2,2048]{2,1,0:T(2,128)(2,1)}), bf16[8,2,2048]{2,1,0:T(2,128)(2,1)S(1)}, u32[]{:S(2)}, u32[]{:S(2)}) %all-to-all-start.2) | async-done | bytes 65568 | tf_op jit(solution)/shard_map/all_to_all | solution.py:116
  36.9 3.3 %all-to-all-start.3 = ((bf16[8,2,2048]{2,1,0:T(2,128)(2,1)}), bf16[8,2,2048]{2,1,0:T(2,128)(2,1)S(1)}, u32[]{:S(2)}, u32[]{:S(2)}) async-start(bf16[8,2,2048]{2,1,0:T(2,128)(2,1)} %reshape.134), calls=%async_computation.3 | async-start | bytes 131072 | tf_op jit(solution)/shard_map/all_to_all | solution.py:14
  40.3 0.1 reshape.133
  40.4 0.1 copy.38
  40.5 0.1 all_to_all.73
  40.7 4.7 %fusion.13 = f32[512,64]{0,1:T(8,128)S(1)} fusion(bf16[512,64]{0,1:T(8,128)(2,1)S(1)} %all_to_all.73), kind=kOutput, calls=%fused_computation.23 | convolution fusion | flops 204996608 | bytes 196608 | tf_op jit(solution)/shard_map/while/body/eval_jaxpr/dot_general | solution.py:74
  45.4 0.7 %all-to-all-done.3 = bf16[8,2,2048]{2,1,0:T(2,128)(2,1)S(1)} async-done(((bf16[8,2,2048]{2,1,0:T(2,128)(2,1)}), bf16[8,2,2048]{2,1,0:T(2,128)(2,1)S(1)}, u32[]{:S(2)}, u32[]{:S(2)}) %all-to-all-start.3) | async-done | bytes 65568 | tf_op jit(solution)/shard_map/all_to_all | solution.py:14
  46.1 0.1 reshape.135
  46.2 4.7 %fusion.5 = bf16[512,64]{0,1:T(8,128)(2,1)S(1)} fusion(f32[512,64]{0,1:T(8,128)S(1)} %fusion.13, bf16[512,64]{1,0:T(8,128)(2,1)S(1)} %bitcast.136), kind=kOutput, calls=%fused_computation.14 | convolution fusion | flops 205094912 | bytes 262144 | tf_op jit(solution)/shard_map/while/body/eval_jaxpr/dot_general | solution.py:80
  51.0 0.1 copy.46
  51.1 0.2 reshape.136
  51.3 10.0 %all_to_all.86 = bf16[8,2,2048]{2,1,0:T(2,128)(2,1)S(1)} all-to-all(bf16[8,2,2048]{2,1,0:T(2,128)(2,1)S(1)} %reshape.136), channel_id=1, replica_groups=mesh['row'=4,'col'=8] {'col'}, dimensions={0} | all-to-all | bytes 131072 | tf_op jit(solution)/shard_map/all_to_all | solution.py:122
  61.3 0.1 reshape.137
  61.5 0.1 copy.40
  61.6 0.1 all_to_all.77
  61.7 7.2 %all_to_all.87 = bf16[4,64,128]{2,1,0:T(8,128)(2,1)S(1)} all-to-all(bf16[4,64,128]{2,1,0:T(8,128)(2,1)S(1)} %all_to_all.77), channel_id=1, replica_groups=mesh['row'=4,'col'=8] {'row'}, dimensions={0} | all-to-all | bytes 131072 | tf_op jit(solution)/shard_map/all_to_all | solution.py:123
  68.9 0.1 copy.41
  69.0 0.0 copy-done
  69.0 0.9 %fusion = bf16[2,64,1024]{2,1,0:T(8,128)(2,1)} fusion(bf16[256,1024]{1,0:T(8,128)(2,1)S(1)} %copy-done, bf16[64,2,256]{2,1,0:T(2,128)(2,1)S(1)} %reshape.122), kind=kOutput, calls=%fused_computation.4 | convolution fusion | flops 67239936 | bytes 851968 | tf_op jit(solution)/shard_map/tsc,cd->std/dot_general | solution.py:127
  (10 shorter events, 0.2 us)
Async XLA Ops:
  0.0 69.0 %copy-start = (bf16[256,1024]{1,0:T(8,128)(2,1)S(1)}, bf16[256,1024]{1,0:T(8,128)(2,1)}, u32[]{:S(2)}) copy-start(bf16[256,1024]{1,0:T(8,128)(2,1)} %param.7) | copy-start | bytes 1572868
  0.0 1.5 %copy-start.2 = (bf16[1024,256]{1,0:T(8,128)(2,1)S(1)}, bf16[1024,256]{1,0:T(8,128)(2,1)}, u32[]{:S(2)}) copy-start(bf16[1024,256]{1,0:T(8,128)(2,1)} %param.5) | copy-start | bytes 1572868
  0.0 1.5 %copy-start.1 = (bf16[2,64,1024]{2,1,0:T(8,128)(2,1)S(1)}, bf16[2,64,1024]{2,1,0:T(8,128)(2,1)}, u32[]{:S(2)}) copy-start(bf16[2,64,1024]{2,1,0:T(8,128)(2,1)} %param.4) | copy-start | bytes 786436
  5.4 10.0 %all-to-all-start = ((bf16[4,2,4096]{2,1,0:T(2,128)(2,1)}), bf16[4,2,4096]{2,1,0:T(2,128)(2,1)S(1)}, u32[]{:S(2)}, u32[]{:S(2)}) async-start(bf16[4,2,4096]{2,1,0:T(2,128)(2,1)} %reshape.130), calls=%async_computation | async-start | bytes 131072 | tf_op jit(solution)/shard_map/all_to_all | solution.py:111
  15.4 8.1 %all-to-all-start.1 = ((bf16[4,2,4096]{2,1,0:T(2,128)(2,1)}), bf16[4,2,4096]{2,1,0:T(2,128)(2,1)S(1)}, u32[]{:S(2)}, u32[]{:S(2)}) async-start(bf16[4,2,4096]{2,1,0:T(2,128)(2,1)} %reshape.128), calls=%async_computation.1 | async-start | bytes 131072 | tf_op jit(solution)/shard_map/all_to_all | solution.py:112
  26.1 10.8 %all-to-all-start.2 = ((bf16[8,2,2048]{2,1,0:T(2,128)(2,1)}), bf16[8,2,2048]{2,1,0:T(2,128)(2,1)S(1)}, u32[]{:S(2)}, u32[]{:S(2)}) async-start(bf16[8,2,2048]{2,1,0:T(2,128)(2,1)} %reshape.132), calls=%async_computation.2 | async-start | bytes 131072 | tf_op jit(solution)/shard_map/all_to_all | solution.py:116
  36.9 9.2 %all-to-all-start.3 = ((bf16[8,2,2048]{2,1,0:T(2,128)(2,1)}), bf16[8,2,2048]{2,1,0:T(2,128)(2,1)S(1)}, u32[]{:S(2)}, u32[]{:S(2)}) async-start(bf16[8,2,2048]{2,1,0:T(2,128)(2,1)} %reshape.134), calls=%async_computation.3 | async-start | bytes 131072 | tf_op jit(solution)/shard_map/all_to_all | solution.py:14
